TPU v7x, 32 devices: a whole 2x2x4 slice. The times are simulated.
32 devices in a mesh: sp: 8 (over z, x), dp: 4 (over y, core).
Axes of the slice: x: 2, y: 2, z: 4, core: 2. Of those that a mesh axis runs over, the one named last changes fastest.
Arguments:
- stream: bfloat16 [4, 1536, 2048], P('dp', 'sp'), may hold values from -6 to 6
- queries: bfloat16 [4, 1536, 2048], P('dp', 'sp'), may hold values from -6 to 6
- key_rows: bfloat16 [4, 1536, 2048], P('dp', 'sp'), may hold values from -6 to 6
- value_rows: bfloat16 [4, 1536, 4096], P('dp', 'sp'), may hold values from -6 to 6
- input_gate: bfloat16 [4, 1536, 16], P('dp', 'sp'), may hold values from -4 to 206
- forget_gate: bfloat16 [4, 1536, 16], P('dp', 'sp'), may hold values from 0 to 12
- head_gain: float32 [16, 256], P('sp'), may hold values from 0.1 to 1.9
- out_weight: bfloat16 [4096, 2048], P('sp'), may hold values from -0.09375 to 0.09375
- mix_gain: float32 [2048], replicated, may hold values from 0.1 to 1.9
- ffn_gain: float32 [2048], replicated, may hold values from 0.1 to 1.9
- final_gain: float32 [2048], replicated, may hold values from 0.1 to 1.9
- expert_ids: int32 [4, 1536, 4], P('dp', 'sp'), may hold values from 0 to 31, all different within a row; in each aligned block of 192 rows (0 to 191, 192 to 383, ..., all dimensions but the last counted through in order) at most 36 rows name the same one
- route_scores: float32 [4, 1536, 4], P('dp', 'sp'), may hold values from 0.05 to 1
- expert_gate: bfloat16 [32, 2048, 512], P(('sp', 'dp')), may hold values from -0.125 to 0.125
- expert_up: bfloat16 [32, 2048, 512], P(('sp', 'dp')), may hold values from -0.125 to 0.125
- expert_down: bfloat16 [32, 512, 2048], P(('sp', 'dp')), may hold values from -0.25 to 0.25
- shared_gate: bfloat16 [2048, 512], replicated, may hold values from -0.125 to 0.125
- shared_up: bfloat16 [2048, 512], replicated, may hold values from -0.125 to 0.125
- shared_down: bfloat16 [512, 2048], replicated, may hold values from -0.25 to 0.25
Outputs:
- updated: bfloat16 [4, 1536, 2048], P('dp', 'sp')
Inputs may be any that keep to these rules, and one draw needn't show every extreme that they name: `expert_ids`: each token names 4 different experts. Among the tokens of one device no expert is named by more than 36 tokens, a bound that some block reaches of some device.
All inputs are finite; a program needn't handle non-finite values.
Results may differ from a plain program's by a relative error of at most 0.006.
Values may be sent and summed in bfloat16 or wider, within the bound.
No kernel may reach another device: no remote copies, remote signals or barrier semaphores. Data moves between devices by JAX's collectives and lax.ppermute only.
A program may use at most 128 MiB of HBM per device.

v0:
```python
import jax
import jax.numpy as jnp
from jax import lax
from jax.sharding import PartitionSpec as P

BLOCK = 256
EPSILON = 1e-06
ROUTE_BOOST = 2.5
HIGHEST = lax.Precision.HIGHEST


def root_norm(values, gains):
    return values * lax.rsqrt(jnp.mean(values * values, axis=-1, keepdims=True) + EPSILON) * gains


def cell_block(carry, pieces):
    state, normal, stabilizer = carry
    query_part, key_part, value_part, gate_part, decay_part = pieces
    length = query_part.shape[1]
    causal = jnp.tril(jnp.ones((length, length), dtype=bool))
    cumulative = jnp.cumsum(decay_part, axis=-1)
    logits = jnp.where(
        causal[None],
        cumulative[:, :, None] - cumulative[:, None, :] + gate_part[:, None, :],
        -jnp.inf,
    )
    peak = jnp.maximum(cumulative + stabilizer[:, None], jnp.max(logits, axis=-1))
    weights = jnp.exp(logits - peak[:, :, None])
    scores = jnp.einsum("hld,hsd->hls", query_part, key_part, precision=HIGHEST) * weights
    carried = jnp.exp(cumulative + stabilizer[:, None] - peak)
    numerator = jnp.einsum("hls,hsv->hlv", scores, value_part, precision=HIGHEST) + carried[
        :, :, None
    ] * jnp.einsum("hvd,hld->hlv", state, query_part, precision=HIGHEST)
    denominator = jnp.sum(scores, axis=-1) + carried * jnp.einsum(
        "hd,hld->hl", normal, query_part, precision=HIGHEST
    )
    result = numerator / jnp.maximum(jnp.abs(denominator), jnp.exp(-peak))[:, :, None]
    block_end = cumulative[:, -1]
    write_log = block_end[:, None] - cumulative + gate_part
    peak_next = jnp.maximum(block_end + stabilizer, jnp.max(write_log, axis=-1))
    decay_all = jnp.exp(block_end + stabilizer - peak_next)
    written = jnp.exp(write_log - peak_next[:, None])[:, :, None] * key_part
    state = decay_all[:, None, None] * state + jnp.einsum(
        "hlv,hld->hvd", value_part, written, precision=HIGHEST
    )
    normal = decay_all[:, None] * normal + jnp.sum(written, axis=1)
    return ((state, normal, peak_next), result)


def memory_cell(queries, key_rows, value_rows, input_gate, forget_gate):
    length, head_count = (queries.shape[0], queries.shape[1])
    key_width = queries.shape[2]
    value_width = value_rows.shape[2]
    blocks = length // BLOCK

    def to_blocks(tensor):
        shaped = tensor.astype(jnp.float32).reshape((blocks, BLOCK, head_count) + tensor.shape[2:])
        return jnp.moveaxis(shaped, 2, 1)

    decay_log = jax.nn.log_sigmoid(forget_gate.astype(jnp.float32))
    start_state = (
        jnp.zeros((head_count, value_width, key_width), jnp.float32),
        jnp.zeros((head_count, key_width), jnp.float32),
        jnp.zeros((head_count,), jnp.float32),
    )
    pieces = (
        to_blocks(queries),
        to_blocks(key_rows) * key_width ** (-0.5),
        to_blocks(value_rows),
        to_blocks(input_gate),
        to_blocks(decay_log),
    )
    _, outputs = lax.scan(cell_block, start_state, pieces)
    return jnp.moveaxis(outputs, 1, 2).reshape(length, head_count, value_width)


def local(
    stream,
    queries,
    key_rows,
    value_rows,
    input_gate,
    forget_gate,
    head_gain,
    out_weight,
    mix_gain,
    ffn_gain,
    final_gain,
    expert_ids,
    route_scores,
    expert_gate,
    expert_up,
    expert_down,
    shared_gate,
    shared_up,
    shared_down,
):
    token_count = stream.shape[1]
    model_width = stream.shape[2]
    head_count = head_gain.shape[0]
    value_width = head_gain.shape[1]
    head_queries, head_keys, head_values, head_input, head_forget = (
        lax.all_to_all(queries, "sp", split_axis=2, concat_axis=1, tiled=True),
        lax.all_to_all(key_rows, "sp", split_axis=2, concat_axis=1, tiled=True),
        lax.all_to_all(value_rows, "sp", split_axis=2, concat_axis=1, tiled=True),
        lax.all_to_all(input_gate, "sp", split_axis=2, concat_axis=1, tiled=True),
        lax.all_to_all(forget_gate, "sp", split_axis=2, concat_axis=1, tiled=True),
    )
    length = head_input.shape[1]
    cell_out = memory_cell(
        head_queries[0].reshape(length, head_count, -1),
        head_keys[0].reshape(length, head_count, -1),
        head_values[0].reshape(length, head_count, value_width),
        head_input[0],
        head_forget[0],
    )
    normed = (
        root_norm(cell_out, head_gain)
        .astype(jnp.bfloat16)
        .reshape(1, length, head_count * value_width)
    )
    token_rows = lax.all_to_all(normed, "sp", split_axis=1, concat_axis=2, tiled=True)[0]
    mixer_out = jnp.dot(
        token_rows,
        lax.all_gather(out_weight, "sp", axis=0, tiled=True),
        preferred_element_type=jnp.float32,
    )
    residual = stream[0].astype(jnp.float32) + root_norm(mixer_out, mix_gain)
    ffn_input = root_norm(residual, ffn_gain).astype(jnp.bfloat16)
    top_count = expert_ids.shape[2]
    local_count = expert_gate.shape[0]
    expert_count = lax.axis_size("sp") * lax.axis_size("dp") * local_count
    capacity = max(2, 3 * token_count * top_count // (2 * expert_count))
    route_ids = expert_ids[0].reshape(-1)
    chosen = (route_ids[:, None] == jnp.arange(expert_count, dtype=jnp.int32)[None, :]).astype(
        jnp.int32
    )
    before = jnp.sum((jnp.cumsum(chosen, axis=0) - chosen) * chosen, axis=1)
    slot_index = route_ids * capacity + before
    slot_owner = jnp.full((expert_count * capacity,), -1, jnp.int32)
    slot_owner = slot_owner.at[slot_index].set(jnp.arange(token_count * top_count, dtype=jnp.int32))
    filled = slot_owner >= 0
    source = jnp.where(filled, slot_owner // top_count, 0)
    outgoing = jnp.where(filled[:, None], ffn_input[source], jnp.zeros((), jnp.bfloat16))
    outgoing = outgoing.reshape(expert_count, capacity, model_width)
    slot_rows = lax.all_to_all(outgoing, ("sp", "dp"), split_axis=0, concat_axis=0, tiled=True)
    shaped = slot_rows.reshape(-1, local_count, slot_rows.shape[1], model_width)
    gate_proj = jnp.einsum(
        "nlcd,ldf->nlcf", shaped, expert_gate, preferred_element_type=jnp.float32
    )
    up_proj = jnp.einsum("nlcd,ldf->nlcf", shaped, expert_up, preferred_element_type=jnp.float32)
    hidden = (jax.nn.silu(gate_proj) * up_proj).astype(jnp.bfloat16)
    answer = jnp.einsum("nlcf,lfd->nlcd", hidden, expert_down, preferred_element_type=jnp.float32)
    expert_out = answer.astype(jnp.bfloat16).reshape(slot_rows.shape)
    returned = lax.all_to_all(expert_out, ("sp", "dp"), split_axis=0, concat_axis=0, tiled=True)
    answers = returned.reshape(expert_count * capacity, model_width)[slot_index]
    answers = answers.reshape(token_count, top_count, model_width)
    scores = route_scores[0]
    route_share = scores / jnp.sum(scores, axis=1, keepdims=True) * ROUTE_BOOST
    routed = jnp.zeros((token_count, model_width), jnp.float32)
    for column in range(top_count):
        routed = routed + route_share[:, column][:, None] * answers[:, column].astype(jnp.float32)
    shared_hidden = (
        jax.nn.silu(jnp.dot(ffn_input, shared_gate, preferred_element_type=jnp.float32))
        * jnp.dot(ffn_input, shared_up, preferred_element_type=jnp.float32)
    ).astype(jnp.bfloat16)
    shared_out = jnp.dot(shared_hidden, shared_down, preferred_element_type=jnp.float32)
    moe_total = routed + shared_out
    result = (residual + root_norm(moe_total, final_gain)).astype(jnp.bfloat16)
    return result[None]


def solution(mesh):
    placed = (
        P("dp", "sp", None),
        P("dp", "sp", None),
        P("dp", "sp", None),
        P("dp", "sp", None),
        P("dp", "sp", None),
        P("dp", "sp", None),
        P("sp", None),
        P("sp", None),
        P(),
        P(),
        P(),
        P("dp", "sp", None),
        P("dp", "sp", None),
        P(("sp", "dp"), None, None),
        P(("sp", "dp"), None, None),
        P(("sp", "dp"), None, None),
        P(),
        P(),
        P(),
    )
    return jax.shard_map(
        local, mesh=mesh, in_specs=placed, out_specs=P("dp", "sp", None), check_vma=False
    )
```

profile of v0, /device:TPU:0, one launch (start us, length us, event | category | flops | bytes accessed | tf_op | source)
XLA Modules:
  0.0 747.4 jit_solution(1196723427909744174)
XLA Ops:
  9.1 7.3 all-to-all-start
  18.3 4.6 all-to-all-done
  22.9 3.3 all-to-all-start.1
  26.2 5.9 copy.84
  32.1 12.6 %reduce.11 = bf16[2048,192]{1,0:T(8,128)(2,1)S(1)} reduce(bf16[2048,1,192]{2,1,0:T(2,128)(2,1)} %bitcast.311, bf16[]{:T(256)} %broadcast.272), dimensions={1}, to_apply=%bitcast.222.reduce_sub_computation | reduce | bytes 1572866
  46.8 6.1 all-to-all-start.3
  52.8 3.8 copy.86
  56.6 12.6 %reduce.12 = bf16[2048,192]{1,0:T(8,128)(2,1)S(1)} reduce(bf16[2048,1,192]{2,1,0:T(2,128)(2,1)} %bitcast.312, bf16[]{:T(256)} %broadcast.272), dimensions={1}, to_apply=%bitcast.216.reduce_sub_computation | reduce | bytes 1572866
  71.5 5.7 all-to-all-start.4
  77.9 9.9 %copy.82 = bf16[1,192,4096]{1,0,2:T(2,128)(2,1)} copy(bf16[1,192,4096]{2,1,0:T(8,128)(2,1)} %param.24) | data formatting | bytes 3145728 | tf_op args[3]
  87.9 25.0 %reduce.10 = bf16[4096,192]{1,0:T(8,128)(2,1)} reduce(bf16[4096,1,192]{2,1,0:T(2,128)(2,1)} %bitcast.303, bf16[]{:T(256)} %broadcast.272), dimensions={1}, to_apply=%bitcast.214.reduce_sub_computation | reduce | bytes 3145730
  112.8 6.7 reshape.420
  119.5 6.1 all-to-all-start.2
  126.0 5.9 reshape.429
  131.9 5.3 convert_multiply_fusion
  137.2 5.9 copy.85
  146.0 3.7 reshape.423
  149.7 5.9 copy.87
  158.6 38.3 %all-to-all-done.2 = bf16[8,2,49152]{2,1,0:T(2,128)(2,1)} async-done(((bf16[8,2,49152]{2,1,0:T(2,128)(2,1)}), bf16[8,2,49152]{2,1,0:T(2,128)(2,1)}, u32[]{:S(2)}, u32[]{:S(2)}) %all-to-all-start.2) | async-done | bytes 1572896 | tf_op jit(solution)/shard_map/all_to_all | solution.py:105
  196.9 7.2 reshape.421
  204.1 10.8 %copy.83 = f32[1,192,8,512]{3,1,2,0:T(8,128)} copy(bf16[1,192,8,512]{1,0,3,2:T(2,128)(2,1)} %bitcast.302) | data formatting | bytes 4718592 | tf_op jit(solution)/shard_map/transpose | solution.py:58
  215.0 5.2 reshape.378
  220.2 82.9 %while.17 = (s32[]{:T(128)}, f32[2,256,128]{2,1,0:T(8,128)}, f32[2,128]{1,0:T(2,128)S(1)}, f32[2]{0:T(128)S(1)}, f32[6,2,256,256]{3,2,1,0:T(8,128)}, /*index=5*/...) while((s32[]{:T(128)}, f32[2,256,128]{2,1,0:T(8,128)}, ...), condition=%wide.region_7.8_spmd.clone, body=%wide.region_0.7_spmd.clone.sunk | while | flops 1009719296 | bytes 9456510 | solution.py:73
  308.9 5.7 mul.238
  314.6 6.0 copy.93
  320.7 5.5 reshape.364
  326.2 3.7 multiply_convert_fusion
  329.9 14.1 %copy.176 = bf16[1,1536,512]{2,0,1:T(2,128)(2,1)} copy(bf16[1,1536,512]{2,1,0:T(8,128)(2,1)S(1)} %multiply_convert_fusion) | data formatting | bytes 3145728 | tf_op jit(solution)/shard_map/convert_element_type | solution.py:119
  344.0 12.0 %reduce.13 = bf16[1536,512]{1,0:T(8,128)(2,1)} reduce(bf16[1536,1,512]{2,1,0:T(2,128)(2,1)} %bitcast.306, bf16[]{:T(256)} %broadcast.272), dimensions={1}, to_apply=%bitcast.255.reduce_sub_computation | reduce | bytes 3145730
  356.0 4.1 reshape.430
  360.1 4.4 all-to-all-start.5
  367.4 3.4 scatter_custom_fusion
  370.9 28.7 %all-to-all-done.5 = bf16[8,2,49152]{2,1,0:T(2,128)(2,1)} async-done(((bf16[8,2,49152]{2,1,0:T(2,128)(2,1)}), bf16[8,2,49152]{2,1,0:T(2,128)(2,1)}, u32[]{:S(2)}, u32[]{:S(2)}) %all-to-all-start.5) | async-done | bytes 1572896 | tf_op jit(solution)/shard_map/all_to_all | solution.py:122
  399.6 6.7 reshape.431
  410.0 8.2 %multiply_reduce_fusion.3 = (f32[192]{0:T(256)S(1)}, f32[192,2048]{1,0:T(8,128)S(1)}) fusion(bf16[192,4096]{1,0:T(8,128)(2,1)} %bitcast.318, bf16[4096,2048]{1,0:T(8,128)(2,1)} %all-gather.2.cloned.1.call-done), kind=kOutput, calls=%fused_computation.78 | convolution fusion | flops 3222011648 | bytes 19923712 | tf_op jit(solution)/shard_map/dot_general | solution.py:123
  419.9 6.0 gather_fusion
  425.8 7.2 gather.9
  436.0 119.3 %all_to_all.70 = bf16[32,36,2048]{2,1,0:T(8,128)(2,1)S(1)} all-to-all(bf16[32,36,2048]{2,1,0:T(8,128)(2,1)S(1)} %broadcast_select_fusion.2), channel_id=1, replica_groups=mesh['sp'=8,'dp'=4] {'sp','dp'}, dimensions={0} | all-to-all | bytes 9437184 | tf_op jit(solution)/shard_map/all_to_all | solution.py:146
  557.6 4.5 fusion.24
  562.1 10.6 %convolution_convert_fusion = bf16[32,36,2048]{2,1,0:T(8,128)(2,1)} fusion(bf16[1,512,2048]{2,1,0:T(8,128)(2,1)S(1)} %copy-done, f32[32,36,512]{2,1,0:T(8,128)} %fusion.24, bf16[32,36,2048]{2,1,0:T(8,128)(2,1)} %copy-done.3, bf16[1,2048,512]{2,1,0:T(8,128)(2,1)} %param.34), kind=kOutput, calls=%fused_computation.49 | convolution fusion | flops 4837736448 | bytes 15990784 | tf_op jit(solution)/shard_map/nlcf,lfd->nlcd/dot_general | solution.py:153
  572.7 4.0 all-to-all-start.7
  578.9 114.7 %all-to-all-done.7 = bf16[32,36,2048]{2,1,0:T(8,128)(2,1)} async-done(((bf16[32,36,2048]{2,1,0:T(8,128)(2,1)}), bf16[32,36,2048]{2,1,0:T(8,128)(2,1)}, u32[]{:S(2)}, u32[]{:S(2)}) %all-to-all-start.7) | async-done | bytes 4718624 | tf_op jit(solution)/shard_map/all_to_all | solution.py:155
  693.6 7.2 reshape.370
  700.9 10.0 %gather_fusion.1 = bf16[768,2048]{1,0:T(8,128)(2,1)} fusion(bf16[1152,2048]{1,0:T(8,128)(2,1)} %reshape.370, s32[1024]{0:T(1024)S(1)} %pad_clamp_fusion.1), kind=kCustom, calls=%fused_computation.1 | custom fusion | bytes 6294528 | tf_op jit(solution)/shard_map/gather | solution.py:156
  710.9 5.7 reshape.371
  716.6 12.3 %fusion.64 = (bf16[192,1,2048]{2,1,0:T(2,128)(2,1)}, bf16[192,1,2048]{2,1,0:T(2,128)(2,1)}, bf16[192,1,2048]{2,1,0:T(2,128)(2,1)}, bf16[192,1,2048]{2,1,0:T(2,128)(2,1)}) fusion(bf16[192,4,2048]{2,1,0:T(4,128)(2,1)} %reshape.371), kind=kLoop, calls=%fused_computation.135 | loop fusion | bytes 6291456 | tf_op jit(solution)/shard_map/slice | solution.py:162
  728.9 8.0 %multiply_reduce_fusion.1 = (f32[192]{0:T(256)S(1)}, f32[192,2048]{1,0:T(8,128)}) fusion(bf16[512,2048]{1,0:T(8,128)(2,1)} %param.39, bf16[192,2048]{1,0:T(8,128)(2,1)S(1)} %multiply_convert_fusion.1, bf16[2048,512]{1,0:T(8,128)(2,1)} %param.38, f32[192,512]{1,0:T(8,128)S(1)} %fusion.66, bf16[192,1,2048]{2,1,0:T(2,128)(2,1)} %get-tuple-element.159, ...), kind=kOutput, calls=%fused_computation.75 | convolution fusion | flops 811401024 | bytes 10096384 | tf_op jit(solution)/shard_map/dot_general | solution.py:167
  736.9 3.4 fusion.37
  (244 shorter events, 119.8 us)
Async XLA Ops:
  6.5 555.6 %copy-start = (bf16[1,512,2048]{2,1,0:T(8,128)(2,1)S(1)}, bf16[1,512,2048]{2,1,0:T(8,128)(2,1)}, u32[]{:S(2)}) copy-start(bf16[1,512,2048]{2,1,0:T(8,128)(2,1)} %param.36) | copy-start | bytes 6291460
  9.1 13.8 %all-to-all-start = ((bf16[8,2,192]{2,1,0:T(2,128)(2,1)}), bf16[8,2,192]{2,1,0:T(2,128)(2,1)S(1)}, u32[]{:S(2)}, u32[]{:S(2)}) async-start(bf16[8,2,192]{2,1,0:T(2,128)(2,1)} %reshape.424), calls=%async_computation | async-start | bytes 16384 | tf_op jit(solution)/shard_map/all_to_all | solution.py:107
  22.9 23.9 %all-to-all-start.1 = ((bf16[8,2,192]{2,1,0:T(2,128)(2,1)}), bf16[8,2,192]{2,1,0:T(2,128)(2,1)S(1)}, u32[]{:S(2)}, u32[]{:S(2)}) async-start(bf16[8,2,192]{2,1,0:T(2,128)(2,1)} %reshape.426), calls=%async_computation.1 | async-start | bytes 16384 | tf_op jit(solution)/shard_map/all_to_all | solution.py:106
  46.8 6.1 copy-start.4
  46.8 24.7 %all-to-all-start.3 = ((bf16[8,2,24576]{2,1,0:T(2,128)(2,1)}), bf16[8,2,24576]{2,1,0:T(2,128)(2,1)}, u32[]{:S(2)}, u32[]{:S(2)}) async-start(bf16[8,2,24576]{2,1,0:T(2,128)(2,1)} %reshape.428), calls=%async_computation.3 | async-start | bytes 1572864 | tf_op jit(solution)/shard_map/all_to_all | solution.py:104
  71.5 48.1 %all-to-all-start.4 = ((bf16[8,2,24576]{2,1,0:T(2,128)(2,1)}), bf16[8,2,24576]{2,1,0:T(2,128)(2,1)S(1)}, u32[]{:S(2)}, u32[]{:S(2)}) async-start(bf16[8,2,24576]{2,1,0:T(2,128)(2,1)} %reshape.422), calls=%async_computation.4 | async-start | bytes 1572864 | tf_op jit(solution)/shard_map/all_to_all | solution.py:103
  77.2 332.8 %all-gather.2.cloned.1.call-start = ((), (), s32[]{:S(2)}) async-start(), calls=%async_computation.8 | async-start | bytes 18874368 | tf_op jit(solution)/shard_map/all_gather | solution.py:125
  119.5 6.2 copy-start.10
  119.5 77.4 %all-to-all-start.2 = ((bf16[8,2,49152]{2,1,0:T(2,128)(2,1)}), bf16[8,2,49152]{2,1,0:T(2,128)(2,1)}, u32[]{:S(2)}, u32[]{:S(2)}) async-start(bf16[8,2,49152]{2,1,0:T(2,128)(2,1)} %reshape.420), calls=%async_computation.2 | async-start | bytes 3145728 | tf_op jit(solution)/shard_map/all_to_all | solution.py:105
  360.1 4.4 copy-start.6
  360.1 39.5 %all-to-all-start.5 = ((bf16[8,2,49152]{2,1,0:T(2,128)(2,1)}), bf16[8,2,49152]{2,1,0:T(2,128)(2,1)}, u32[]{:S(2)}, u32[]{:S(2)}) async-start(bf16[8,2,49152]{2,1,0:T(2,128)(2,1)} %reshape.430), calls=%async_computation.5 | async-start | bytes 3145728 | tf_op jit(solution)/shard_map/all_to_all | solution.py:122
  410.0 8.2 %copy-start.2 = (bf16[1,192,2048]{2,1,0:T(8,128)(2,1)S(1)}, bf16[1,192,2048]{2,1,0:T(8,128)(2,1)}, u32[]{:S(2)}) copy-start(bf16[1,192,2048]{2,1,0:T(8,128)(2,1)} %param.21) | copy-start | bytes 2359300
  410.0 8.3 %copy-start.5 = (f32[2048]{0:T(1024)S(1)}, f32[2048]{0:T(1024)}, u32[]{:S(2)}) copy-start(f32[2048]{0:T(1024)} %param.29) | copy-start | bytes 24580
  418.2 1.2 copy-start.1
  418.3 1.1 copy-start.8
  436.0 121.7 %copy-start.11 = (bf16[1,2048,512]{2,1,0:T(8,128)(2,1)S(1)}, bf16[1,2048,512]{2,1,0:T(8,128)(2,1)}, u32[]{:S(2)}) copy-start(bf16[1,2048,512]{2,1,0:T(8,128)(2,1)} %param.35) | copy-start | bytes 6291460
  555.3 2.3 copy-start.3
  572.7 4.0 copy-start.7
  572.7 121.0 %all-to-all-start.7 = ((bf16[32,36,2048]{2,1,0:T(8,128)(2,1)}), bf16[32,36,2048]{2,1,0:T(8,128)(2,1)}, u32[]{:S(2)}, u32[]{:S(2)}) async-start(bf16[32,36,2048]{2,1,0:T(8,128)(2,1)} %convolution_convert_fusion), calls=%async_computation.7 | async-start | bytes 10485760 | tf_op jit(solution)/shard_map/all_to_all | solution.py:155
  728.9 8.0 %copy-start.9 = (f32[2048]{0:T(1024)S(1)}, f32[2048]{0:T(1024)}, u32[]{:S(2)}) copy-start(f32[2048]{0:T(1024)} %param.31) | copy-start | bytes 24580
Sparse Core Ops, SparseCore 0:
  80.1 262.0 all-gather.1
where the time goes:
time: 758 us; the launch traced here: 747 us
  local copies, waits for them, and re-layouts  207 us (27%)
  waiting for transfers between devices  187 us (25%)
  blocking collectives  119 us (16%)
  other arithmetic  94.6 us (12%)
  matrix products  88.1 us (12%)
  starting transfers between devices  37.2 us (5%)
  between operations  14 us (2%)
    all_to_all x1, blocking collectives, local(): lax.all_to_all(outgoing, ('sp', 'dp'), split_axis=0, concat_axis=0, tiled...  119 us
    all_to_all x1, waiting for transfers between devices, local(): lax.all_to_all(expert_out, ('sp', 'dp'), split_axis=0, concat_axis=0, til...  115 us
    unnamed x46, local copies, waits for them, and re-layouts  68.2 us
    unnamed x9, other arithmetic  63.3 us
    all_to_all x1, waiting for transfers between devices, local(): lax.all_to_all(value_rows, 'sp', split_axis=2, concat_axis=1, tiled=True)  38.3 us
    all_to_all x1, waiting for transfers between devices, local(): lax.all_to_all(normed, 'sp', split_axis=1, concat_axis=2, tiled=True)[0]  28.7 us
    transpose x6, local copies, waits for them, and re-layouts, to_blocks(): return jnp.moveaxis(shaped, 2, 1)  25 us
    dot_general x6, matrix products, cell_block(): jnp.einsum('hls,hsv->hlv', scores, value_part, precision=HIGHEST)  18.1 us
  transfers between devices with their start and end apart: 8, of which 5 were waited for; matrix products, arithmetic and copies ran while one was open for 40% of the time, Pallas kernels for 0%

commit v1 on v0

--- a/solution.py
+++ b/solution.py
@@ -102,7 +102,12 @@
     head_queries, head_keys, head_values, head_input, head_forget = (
         lax.all_to_all(queries, "sp", split_axis=2, concat_axis=1, tiled=True),
         lax.all_to_all(key_rows, "sp", split_axis=2, concat_axis=1, tiled=True),
-        lax.all_to_all(value_rows, "sp", split_axis=2, concat_axis=1, tiled=True),
+        jnp.concatenate(
+            lax.all_to_all(
+                jnp.stack(jnp.split(value_rows, lax.axis_size("sp"), axis=2)), "sp", 0, 0
+            ),
+            axis=1,
+        ),
         lax.all_to_all(input_gate, "sp", split_axis=2, concat_axis=1, tiled=True),
         lax.all_to_all(forget_gate, "sp", split_axis=2, concat_axis=1, tiled=True),
     )

time: 758 us -> 735 us (0.970)
  waiting for transfers between devices: 187 us -> 212 us
  other arithmetic: 94.6 us -> 70.4 us
  local copies, waits for them, and re-layouts: 207 us -> 185 us
    all_to_all x1, waiting for transfers between devices: 0.01 us -> 31.9 us  [local(): lax.all_to_all(queries, 'sp', split_axis=2, concat_axis=1, tiled=True)]
    unnamed x9 -> x8, other arithmetic: 63.3 us -> 39 us
    unnamed x46 -> x50, local copies, waits for them, and re-layouts: 68.2 us -> 55.8 us
    transpose x6 -> x5, local copies, waits for them, and re-layouts: 25 us -> 13.7 us  [to_blocks(): return jnp.moveaxis(shaped, 2, 1)]
    all_to_all x1, waiting for transfers between devices: 38.3 us -> 29.4 us  [local(): lax.all_to_all(jnp.stack(jnp.split(value_rows, lax.axis_size('sp'), axis=...]
  transfers between devices with their start and end apart: 8 -> 8, of which waited for: 5 -> 5; matrix products, arithmetic and copies ran while one was open for 40% -> 35% of each run, Pallas kernels for 0% -> 0%
where the time goes in v1:
time: 735 us; the launch traced here: 725 us
  waiting for transfers between devices  212 us (29%)
  local copies, waits for them, and re-layouts  185 us (25%)
  blocking collectives  120 us (16%)
  matrix products  88.1 us (12%)
  other arithmetic  70.4 us (10%)
  starting transfers between devices  35.6 us (5%)
  between operations  14 us (2%)
    all_to_all x1, blocking collectives, local(): lax.all_to_all(outgoing, ('sp', 'dp'), split_axis=0, concat_axis=0, tiled...  120 us
    all_to_all x1, waiting for transfers between devices, local(): lax.all_to_all(expert_out, ('sp', 'dp'), split_axis=0, concat_axis=0, til...  115 us
    unnamed x50, local copies, waits for them, and re-layouts  55.8 us
    unnamed x8, other arithmetic  39 us
    all_to_all x1, waiting for transfers between devices, local(): lax.all_to_all(queries, 'sp', split_axis=2, concat_axis=1, tiled=True)  31.9 us
    all_to_all x1, waiting for transfers between devices, local(): lax.all_to_all(normed, 'sp', split_axis=1, concat_axis=2, tiled=True)[0]  30.8 us
    all_to_all x1, waiting for transfers between devices, local(): lax.all_to_all(jnp.stack(jnp.split(value_rows, lax.axis_size('sp'), axis=...  29.4 us
    dot_general x6, matrix products, cell_block(): jnp.einsum('hls,hsv->hlv', scores, value_part, precision=HIGHEST)  18.1 us
  transfers between devices with their start and end apart: 8, of which 5 were waited for; matrix products, arithmetic and copies ran while one was open for 35% of the time, Pallas kernels for 0%

profile of v1, /device:TPU:0, one launch (start us, length us, event | category | flops | bytes accessed | tf_op | source)
XLA Modules:
  0.0 724.9 jit_solution(11350512026748193744)
XLA Ops:
  9.3 7.3 %all-to-all-start = ((bf16[8,2,192]{2,1,0:T(2,128)(2,1)}), bf16[8,2,192]{2,1,0:T(2,128)(2,1)S(1)}, u32[]{:S(2)}, u32[]{:S(2)}) async-start(bf16[8,2,192]{2,1,0:T(2,128)(2,1)} %reshape.418), calls=%async_computation | async-start | bytes 16384 | tf_op jit(solution)/shard_map/all_to_all | solution.py:112
  18.7 4.5 all-to-all-done
  23.1 3.3 all-to-all-start.1
  26.5 5.9 copy.79
  32.4 12.7 %reduce.10 = bf16[2048,192]{1,0:T(8,128)(2,1)S(1)} reduce(bf16[2048,1,192]{2,1,0:T(2,128)(2,1)} %bitcast.319, bf16[]{:T(256)} %broadcast.272), dimensions={1}, to_apply=%bitcast.233.reduce_sub_computation | reduce | bytes 1572866
  47.1 6.1 all-to-all-start.3
  53.9 3.8 copy.81
  57.7 12.7 %reduce.11 = bf16[2048,192]{1,0:T(8,128)(2,1)S(1)} reduce(bf16[2048,1,192]{2,1,0:T(2,128)(2,1)} %bitcast.320, bf16[]{:T(256)} %broadcast.272), dimensions={1}, to_apply=%bitcast.227.reduce_sub_computation | reduce | bytes 1572866
  75.7 6.0 all-to-all-start.4
  91.4 31.9 %all-to-all-done.4 = bf16[8,2,24576]{2,1,0:T(2,128)(2,1)S(1)} async-done(((bf16[8,2,24576]{2,1,0:T(2,128)(2,1)}), bf16[8,2,24576]{2,1,0:T(2,128)(2,1)S(1)}, u32[]{:S(2)}, u32[]{:S(2)}) %all-to-all-start.4) | async-done | bytes 786464 | tf_op jit(solution)/shard_map/all_to_all | solution.py:103
  123.4 4.5 all-to-all-start.2
  128.2 5.9 reshape.423
  134.1 5.3 convert_multiply_fusion
  139.4 5.9 copy.80
  148.2 3.7 reshape.417
  151.9 6.0 copy.82
  160.9 29.4 %all-to-all-done.2 = bf16[8,1,192,512]{3,2,1,0:T(8,128)(2,1)} async-done(((bf16[8,1,192,512]{3,2,1,0:T(8,128)(2,1)}), bf16[8,1,192,512]{3,2,1,0:T(8,128)(2,1)}, u32[]{:S(2)}, u32[]{:S(2)}) %all-to-all-start.2) | async-done | bytes 1572896 | tf_op jit(solution)/shard_map/all_to_all | solution.py:106
  190.2 4.7 reshape.375
  194.9 82.9 %while.17 = (s32[]{:T(128)}, f32[2,256,128]{2,1,0:T(8,128)}, f32[2,128]{1,0:T(2,128)S(1)}, f32[2]{0:T(128)S(1)}, f32[6,2,256,256]{3,2,1,0:T(8,128)}, /*index=5*/...) while((s32[]{:T(128)}, f32[2,256,128]{2,1,0:T(8,128)}, ...), condition=%wide.region_7.8_spmd.clone, body=%wide.region_0.7_spmd.clone.sunk | while | flops 1009719296 | bytes 9456510 | solution.py:73
  216.0 3.0 fusion.103
  244.2 3.0 fusion.103
  272.4 3.0 fusion.103
  280.5 3.3 mul.237
  283.8 5.7 mul.238
  289.6 6.0 copy.88
  295.6 5.5 reshape.361
  301.1 3.7 multiply_convert_fusion
  304.8 14.1 %copy.171 = bf16[1,1536,512]{2,0,1:T(2,128)(2,1)} copy(bf16[1,1536,512]{2,1,0:T(8,128)(2,1)S(1)} %multiply_convert_fusion) | data formatting | bytes 3145728 | tf_op jit(solution)/shard_map/convert_element_type | solution.py:124
  318.9 12.2 %reduce.12 = bf16[1536,512]{1,0:T(8,128)(2,1)} reduce(bf16[1536,1,512]{2,1,0:T(2,128)(2,1)} %bitcast.314, bf16[]{:T(256)} %broadcast.272), dimensions={1}, to_apply=%bitcast.266.reduce_sub_computation | reduce | bytes 3145730
  331.1 4.1 reshape.424
  335.2 4.4 all-to-all-start.5
  342.4 3.4 scatter_custom_fusion
  346.0 30.8 %all-to-all-done.5 = bf16[8,2,49152]{2,1,0:T(2,128)(2,1)} async-done(((bf16[8,2,49152]{2,1,0:T(2,128)(2,1)}), bf16[8,2,49152]{2,1,0:T(2,128)(2,1)}, u32[]{:S(2)}, u32[]{:S(2)}) %all-to-all-start.5) | async-done | bytes 1572896 | tf_op jit(solution)/shard_map/all_to_all | solution.py:127
  376.8 6.7 reshape.425
  387.2 8.2 %multiply_reduce_fusion.3 = (f32[192]{0:T(256)S(1)}, f32[192,2048]{1,0:T(8,128)S(1)}) fusion(bf16[192,4096]{1,0:T(8,128)(2,1)} %bitcast.326, bf16[4096,2048]{1,0:T(8,128)(2,1)} %all-gather.2.cloned.1.call-done), kind=kOutput, calls=%fused_computation.78 | convolution fusion | flops 3222011648 | bytes 19923712 | tf_op jit(solution)/shard_map/dot_general | solution.py:128
  397.0 6.0 gather_fusion
  403.0 7.2 gather.9
  413.1 119.6 %all_to_all.66 = bf16[32,36,2048]{2,1,0:T(8,128)(2,1)S(1)} all-to-all(bf16[32,36,2048]{2,1,0:T(8,128)(2,1)S(1)} %broadcast_select_fusion.2), channel_id=1, replica_groups=mesh['sp'=8,'dp'=4] {'sp','dp'}, dimensions={0} | all-to-all | bytes 9437184 | tf_op jit(solution)/shard_map/all_to_all | solution.py:151
  535.1 4.5 fusion.24
  539.6 10.6 %convolution_convert_fusion = bf16[32,36,2048]{2,1,0:T(8,128)(2,1)} fusion(bf16[1,512,2048]{2,1,0:T(8,128)(2,1)S(1)} %copy-done, f32[32,36,512]{2,1,0:T(8,128)} %fusion.24, bf16[32,36,2048]{2,1,0:T(8,128)(2,1)} %copy-done.3, bf16[1,2048,512]{2,1,0:T(8,128)(2,1)} %param.34), kind=kOutput, calls=%fused_computation.49 | convolution fusion | flops 4837736448 | bytes 15990784 | tf_op jit(solution)/shard_map/nlcf,lfd->nlcd/dot_general | solution.py:158
  550.2 4.0 all-to-all-start.7
  556.4 114.7 %all-to-all-done.7 = bf16[32,36,2048]{2,1,0:T(8,128)(2,1)} async-done(((bf16[32,36,2048]{2,1,0:T(8,128)(2,1)}), bf16[32,36,2048]{2,1,0:T(8,128)(2,1)}, u32[]{:S(2)}, u32[]{:S(2)}) %all-to-all-start.7) | async-done | bytes 4718624 | tf_op jit(solution)/shard_map/all_to_all | solution.py:160
  671.1 7.2 reshape.367
  678.4 10.0 %gather_fusion.1 = bf16[768,2048]{1,0:T(8,128)(2,1)} fusion(bf16[1152,2048]{1,0:T(8,128)(2,1)} %reshape.367, s32[1024]{0:T(1024)S(1)} %pad_clamp_fusion.1), kind=kCustom, calls=%fused_computation.1 | custom fusion | bytes 6294528 | tf_op jit(solution)/shard_map/gather | solution.py:161
  688.4 5.7 reshape.368
  694.1 12.3 %fusion.64 = (bf16[192,1,2048]{2,1,0:T(2,128)(2,1)}, bf16[192,1,2048]{2,1,0:T(2,128)(2,1)}, bf16[192,1,2048]{2,1,0:T(2,128)(2,1)}, bf16[192,1,2048]{2,1,0:T(2,128)(2,1)}) fusion(bf16[192,4,2048]{2,1,0:T(4,128)(2,1)} %reshape.368), kind=kLoop, calls=%fused_computation.143 | loop fusion | bytes 6291456 | tf_op jit(solution)/shard_map/slice | solution.py:167
  706.5 8.0 %multiply_reduce_fusion.1 = (f32[192]{0:T(256)S(1)}, f32[192,2048]{1,0:T(8,128)}) fusion(bf16[512,2048]{1,0:T(8,128)(2,1)} %param.39, bf16[192,2048]{1,0:T(8,128)(2,1)S(1)} %multiply_convert_fusion.1, bf16[2048,512]{1,0:T(8,128)(2,1)} %param.38, f32[192,512]{1,0:T(8,128)S(1)} %fusion.66, bf16[192,1,2048]{2,1,0:T(2,128)(2,1)} %get-tuple-element.159, ...), kind=kOutput, calls=%fused_computation.75 | convolution fusion | flops 811401024 | bytes 10096384 | tf_op jit(solution)/shard_map/dot_general | solution.py:172
  714.4 3.4 fusion.37
  (247 shorter events, 120.6 us)
Async XLA Ops:
  6.5 533.1 %copy-start = (bf16[1,512,2048]{2,1,0:T(8,128)(2,1)S(1)}, bf16[1,512,2048]{2,1,0:T(8,128)(2,1)}, u32[]{:S(2)}) copy-start(bf16[1,512,2048]{2,1,0:T(8,128)(2,1)} %param.36) | copy-start | bytes 6291460
  9.3 13.8 %all-to-all-start = ((bf16[8,2,192]{2,1,0:T(2,128)(2,1)}), bf16[8,2,192]{2,1,0:T(2,128)(2,1)S(1)}, u32[]{:S(2)}, u32[]{:S(2)}) async-start(bf16[8,2,192]{2,1,0:T(2,128)(2,1)} %reshape.418), calls=%async_computation | async-start | bytes 16384 | tf_op jit(solution)/shard_map/all_to_all | solution.py:112
  23.1 24.0 %all-to-all-start.1 = ((bf16[8,2,192]{2,1,0:T(2,128)(2,1)}), bf16[8,2,192]{2,1,0:T(2,128)(2,1)S(1)}, u32[]{:S(2)}, u32[]{:S(2)}) async-start(bf16[8,2,192]{2,1,0:T(2,128)(2,1)} %reshape.420), calls=%async_computation.1 | async-start | bytes 16384 | tf_op jit(solution)/shard_map/all_to_all | solution.py:111
  47.1 6.8 copy-start.4
  47.1 28.6 %all-to-all-start.3 = ((bf16[8,2,24576]{2,1,0:T(2,128)(2,1)}), bf16[8,2,24576]{2,1,0:T(2,128)(2,1)}, u32[]{:S(2)}, u32[]{:S(2)}) async-start(bf16[8,2,24576]{2,1,0:T(2,128)(2,1)} %reshape.422), calls=%async_computation.3 | async-start | bytes 1572864 | tf_op jit(solution)/shard_map/all_to_all | solution.py:104
  53.2 334.0 %all-gather.2.cloned.1.call-start = ((), (), s32[]{:S(2)}) async-start(), calls=%async_computation.8 | async-start | bytes 18874368 | tf_op jit(solution)/shard_map/all_gather | solution.py:130
  75.7 47.7 %all-to-all-start.4 = ((bf16[8,2,24576]{2,1,0:T(2,128)(2,1)}), bf16[8,2,24576]{2,1,0:T(2,128)(2,1)S(1)}, u32[]{:S(2)}, u32[]{:S(2)}) async-start(bf16[8,2,24576]{2,1,0:T(2,128)(2,1)} %reshape.416), calls=%async_computation.4 | async-start | bytes 1572864 | tf_op jit(solution)/shard_map/all_to_all | solution.py:103
  91.4 36.5 %copy-start.10 = (f32[2,256]{1,0:T(2,128)S(1)}, f32[2,256]{1,0:T(2,128)}, u32[]{:S(2)}) copy-start(f32[2,256]{1,0:T(2,128)} %param.27) | copy-start | bytes 6148
  123.4 66.9 %all-to-all-start.2 = ((bf16[8,1,192,512]{3,2,1,0:T(8,128)(2,1)}), bf16[8,1,192,512]{3,2,1,0:T(8,128)(2,1)}, u32[]{:S(2)}, u32[]{:S(2)}) async-start(bf16[8,1,192,512]{3,2,1,0:T(8,128)(2,1)} %bitcast_dynamic-update-slice_fusion), calls=%async_computation.2 | async-start | bytes 3145728 | tf_op jit(solution)/shard_map/all_to_all | solution.py:106
  335.2 4.4 copy-start.6
  335.2 41.6 %all-to-all-start.5 = ((bf16[8,2,49152]{2,1,0:T(2,128)(2,1)}), bf16[8,2,49152]{2,1,0:T(2,128)(2,1)}, u32[]{:S(2)}, u32[]{:S(2)}) async-start(bf16[8,2,49152]{2,1,0:T(2,128)(2,1)} %reshape.424), calls=%async_computation.5 | async-start | bytes 3145728 | tf_op jit(solution)/shard_map/all_to_all | solution.py:127
  387.2 8.3 %copy-start.2 = (bf16[1,192,2048]{2,1,0:T(8,128)(2,1)S(1)}, bf16[1,192,2048]{2,1,0:T(8,128)(2,1)}, u32[]{:S(2)}) copy-start(bf16[1,192,2048]{2,1,0:T(8,128)(2,1)} %param.21) | copy-start | bytes 2359300
  387.2 8.3 %copy-start.5 = (f32[2048]{0:T(1024)S(1)}, f32[2048]{0:T(1024)}, u32[]{:S(2)}) copy-start(f32[2048]{0:T(1024)} %param.29) | copy-start | bytes 24580
  395.4 1.2 copy-start.1
  395.4 1.1 copy-start.8
  413.1 122.0 %copy-start.11 = (bf16[1,2048,512]{2,1,0:T(8,128)(2,1)S(1)}, bf16[1,2048,512]{2,1,0:T(8,128)(2,1)}, u32[]{:S(2)}) copy-start(bf16[1,2048,512]{2,1,0:T(8,128)(2,1)} %param.35) | copy-start | bytes 6291460
  532.8 2.3 copy-start.3
  550.2 4.0 copy-start.7
  550.2 121.0 %all-to-all-start.7 = ((bf16[32,36,2048]{2,1,0:T(8,128)(2,1)}), bf16[32,36,2048]{2,1,0:T(8,128)(2,1)}, u32[]{:S(2)}, u32[]{:S(2)}) async-start(bf16[32,36,2048]{2,1,0:T(8,128)(2,1)} %convolution_convert_fusion), calls=%async_computation.7 | async-start | bytes 10485760 | tf_op jit(solution)/shard_map/all_to_all | solution.py:160
  706.5 8.0 %copy-start.9 = (f32[2048]{0:T(1024)S(1)}, f32[2048]{0:T(1024)}, u32[]{:S(2)}) copy-start(f32[2048]{0:T(1024)} %param.31) | copy-start | bytes 24580
Sparse Core Ops, SparseCore 0:
  56.1 278.0 all-gather.1
